TPU v7x, 128 devices: a whole 4x4x4 slice. The times are simulated.
128 devices in a mesh: kv: 16 (over z, y), tp: 8 (over x, core).
Axes of the slice: x: 4, y: 4, z: 4, core: 2. Of those that a mesh axis runs over, the one named last changes fastest.
Arguments:
- tokens: bfloat16 [48, 24, 4096], P(None, None, 'kv'), may hold values from -6 to 6
- norm_gain: bfloat16 [4096], P('kv'), may hold values from 0.099609375 to 1.8984375
- w_query: bfloat16 [4096, 2048], P('kv', 'tp'), may hold values from -0.09375 to 0.09375
- w_key: bfloat16 [4096, 512], P('kv', 'tp'), may hold values from -0.09375 to 0.09375
- w_value: bfloat16 [4096, 512], P('kv', 'tp'), may hold values from -0.09375 to 0.09375
- w_forget: bfloat16 [4096, 32], replicated, may hold values from -0.09375 to 0.09375
- forget_bias: float32 [32], P('tp'), may hold values from -1 to 3
- query_gain: bfloat16 [64], replicated, may hold values from 0.099609375 to 1.8984375
- key_gain: bfloat16 [64], replicated, may hold values from 0.099609375 to 1.8984375
- w_out: bfloat16 [2048, 4096], P('tp', 'kv'), may hold values from -0.5 to 0.5
- key_cache: bfloat16 [48, 512, 16384], P(None, 'tp', 'kv'), may hold values from -46 to 46
- value_cache: bfloat16 [48, 512, 16384], P(None, 'tp', 'kv'), may hold values from -6 to 6
- gate_sums: float32 [48, 32, 16384], P(None, 'tp', 'kv'), may hold values from -2051 to 0, as said below
- parents: int32 [48, 24], replicated, may hold values from -1 to 22, as said below
- lengths: int32 [48], replicated, may hold values from 8192 to 16378
- accepted: int32 [48], replicated, may hold values from 0 to 6
Outputs:
- mixed: bfloat16 [48, 24, 4096], P(None, None, 'kv')
Inputs may be any that keep to these rules, and one draw needn't show every extreme that they name: `gate_sums`: for each sequence and head it never rises along the positions. `parents`: the parent of proposal i is -1 (the cache's last visible position) or one of the proposals i - 3 to i - 1. The accepted proposals stand in the cache right after the first lengths positions.
All inputs are finite; a program needn't handle non-finite values.
Results may differ from a plain program's by a relative error of at most 0.03.
Values may be sent and summed in bfloat16 or wider, within the bound.
A program may use at most 128 MiB of HBM per device.

v0:
```python
import jax
import jax.numpy as jnp
from jax import lax
from jax.sharding import PartitionSpec as P

eps = 1e-05
floor_value = -1e30


def sent_to_all(shard, axis):
    size = lax.axis_size(axis)
    return lax.all_to_all(
        jnp.broadcast_to(shard[None], (size, *shard.shape)), axis, 0, 0, tiled=True
    )


def of_everyone(shard, axis):
    everything = sent_to_all(shard, axis)
    return jnp.sum(everything, axis=0)


def in_one(arrays, axis):
    vector, at, gathered = (jnp.concatenate([a.reshape(-1) for a in arrays]), 0, [])
    so_far = of_everyone(vector, axis)
    for a in arrays:
        gathered.append(so_far[at : at + a.size].reshape(a.shape))
        at += a.size
    return tuple(gathered)


def in_blocks(shard, dim, size):
    before, after = (shard.shape[:dim], shard.shape[dim + 1 :])
    return jnp.moveaxis(shard.reshape(*before, size, -1, *after), dim, 0)


def summed_on_arrival(shard, axis, dim):
    size = lax.axis_size(axis)
    tiles = lax.all_to_all(in_blocks(shard, dim, size), axis, 0, 0, tiled=True)
    return jnp.sum(tiles.astype(jnp.float32), axis=0)


def joined_along(tiles, dim):
    dims = list(tiles.shape[1:])
    dims[dim] *= tiles.shape[0]
    return jnp.moveaxis(tiles, 0, dim).reshape(dims)


def collect(shard, axis, dim):
    return joined_along(sent_to_all(shard, axis), dim)


def in_one_piece(arrays, axis, split_dim, concat_dim, along):
    ends, at = ([], 0)
    for a in arrays[:-1]:
        at += a.shape[along]
        ends.append(at)
    both = jnp.concatenate(arrays, axis=along)
    return tuple(
        jnp.split(
            lax.all_to_all(both, axis, split_axis=split_dim, concat_axis=concat_dim, tiled=True),
            ends,
            axis=along,
        )
    )


def gathered_total(shard, axis):
    tiles = lax.all_gather(shard, axis).astype(jnp.float32)
    return tiles.sum(axis=0)


def head_norm(block, gain):
    mean_sq = jnp.mean(block * block, axis=-1, keepdims=True)
    return (block * lax.rsqrt(mean_sq + eps) * gain.astype(jnp.float32)).astype(jnp.bfloat16)


def ancestors(parents, node_count):
    node_ids = jnp.arange(node_count, dtype=jnp.int32)
    reach_map = (parents[:, :, None] == node_ids[None, None, :]).astype(jnp.float32)
    reach_map = reach_map + jnp.eye(node_count, dtype=jnp.float32)[None]
    for repeat_index in range(max(node_count - 1, 1).bit_length()):
        reach_map = jnp.minimum(jnp.einsum("bij,bjk->bik", reach_map, reach_map), 1.0)
    return reach_map


def finish(projected, inverse, query_gain, key_gain, local_heads, kv_local):
    row_count = projected.shape[0]
    head_dim = query_gain.shape[0]
    scaled_proj = projected * inverse[:, None]
    query_width = local_heads * head_dim
    key_width = kv_local * head_dim
    query_rows = head_norm(
        scaled_proj[:, :query_width].reshape(row_count, local_heads, head_dim), query_gain
    )
    keys_new = head_norm(
        scaled_proj[:, query_width : query_width + key_width].reshape(
            row_count, kv_local, head_dim
        ),
        key_gain,
    )
    values_new = scaled_proj[:, query_width + key_width :].astype(jnp.bfloat16)
    return jnp.concatenate(
        [
            query_rows.reshape(row_count, query_width),
            keys_new.reshape(row_count, key_width),
            values_new,
        ],
        axis=1,
    )


def body(
    tokens,
    norm_gain,
    w_query,
    w_key,
    w_value,
    w_forget,
    forget_bias,
    query_gain,
    key_gain,
    w_out,
    key_cache,
    value_cache,
    gate_sums,
    parents,
    lengths,
    accepted,
):
    seq_count, drafts, local_width = tokens.shape
    row_count = seq_count * drafts
    head_dim = query_gain.shape[0]
    local_heads = forget_bias.shape[0]
    kv_local = w_key.shape[1] // head_dim
    group_size = local_heads // kv_local
    positions = key_cache.shape[2]
    model_width = local_width * lax.axis_size("kv")
    kv_index = lax.axis_index("kv")
    tp_index = lax.axis_index("tp")
    wide_rows = tokens.reshape(row_count, local_width).astype(jnp.float32)
    squares = jnp.sum(wide_rows * wide_rows, axis=1)
    scaled = (wide_rows * norm_gain.astype(jnp.float32)[None, :]).astype(jnp.bfloat16)
    forget_rows = lax.dynamic_slice(
        w_forget, (kv_index * local_width, tp_index * local_heads), (local_width, local_heads)
    )
    partial_proj = jnp.dot(
        scaled,
        jnp.concatenate([w_query, w_key, w_value], axis=1),
        preferred_element_type=jnp.float32,
    )
    partial_gate = jnp.dot(scaled, forget_rows, preferred_element_type=jnp.float32)
    gate_pre, total_squares = in_one((partial_gate, squares), "kv")
    inverse = lax.rsqrt(total_squares / model_width + eps)
    share = summed_on_arrival(partial_proj.astype(jnp.bfloat16), "kv", 0)
    share_rows = share.shape[0]
    share_inverse = lax.dynamic_slice_in_dim(inverse, kv_index * share_rows, share_rows)
    packed = collect(
        finish(share, share_inverse, query_gain, key_gain, local_heads, kv_local), "kv", 0
    )
    query_width = local_heads * head_dim
    key_width = kv_local * head_dim
    query_rows = packed[:, :query_width].reshape(seq_count, drafts, kv_local, group_size, head_dim)
    keys_new = packed[:, query_width : query_width + key_width].reshape(
        seq_count, drafts, kv_local, head_dim
    )
    values_new = packed[:, query_width + key_width :].reshape(seq_count, drafts, kv_local, head_dim)
    gate_logarithm = jax.nn.log_sigmoid(gate_pre * inverse[:, None] + forget_bias[None, :])
    reach_map = ancestors(parents, drafts)
    path_sums = jnp.einsum(
        "bij,bjh->bhi", reach_map, gate_logarithm.reshape(seq_count, drafts, local_heads)
    )
    valid_len = lengths + accepted
    local_last = valid_len - 1 - kv_index * positions
    is_owner = (local_last >= 0) & (local_last < positions)
    slot_positions = jnp.arange(positions, dtype=jnp.int32)
    gate_last = jnp.sum(
        jnp.where(slot_positions[None, None, :] == local_last[:, None, None], gate_sums, 0.0),
        axis=2,
    )
    cache_mask = slot_positions[None, :] + kv_index * positions < valid_len[:, None]
    scale = head_dim ** (-0.5)
    stored_key_rows = key_cache.reshape(seq_count, kv_local, head_dim, positions)
    cache_values = value_cache.reshape(seq_count, kv_local, head_dim, positions)
    cache_logits = jnp.einsum(
        "oxfzu,ofuq->ofzxq", query_rows, stored_key_rows, preferred_element_type=jnp.float32
    ).reshape(seq_count, local_heads, drafts, positions)
    cache_logits = cache_logits * scale - gate_sums[:, :, None, :]
    new_logits = jnp.einsum(
        "bpkgd,bjkd->bkgpj", query_rows, keys_new, preferred_element_type=jnp.float32
    ).reshape(seq_count, local_heads, drafts, drafts)
    new_logits = new_logits * scale - gate_last[:, :, None, None] - path_sums[:, :, None, :]
    cache_keep = jnp.broadcast_to(cache_mask[:, None, None, :], cache_logits.shape)
    new_keep = jnp.broadcast_to(
        (reach_map[:, None, :, :] > 0.5) & is_owner[:, None, None, None], new_logits.shape
    )
    row_top = jnp.maximum(
        jnp.max(jnp.where(cache_keep, cache_logits, floor_value), axis=3),
        jnp.max(jnp.where(new_keep, new_logits, floor_value), axis=3),
    )
    cache_weights = jnp.where(cache_keep, jnp.exp(cache_logits - row_top[..., None]), 0.0)
    new_weights = jnp.where(new_keep, jnp.exp(new_logits - row_top[..., None]), 0.0)
    row_total = jnp.sum(cache_weights, axis=3) + jnp.sum(new_weights, axis=3)
    weighted = jnp.einsum(
        "ftxwm,ftnm->fwtxn",
        cache_weights.astype(jnp.bfloat16).reshape(
            seq_count, kv_local, group_size, drafts, positions
        ),
        cache_values,
        preferred_element_type=jnp.float32,
    )
    weighted = weighted + jnp.einsum(
        "bkgpj,bjkd->bpkgd",
        new_weights.astype(jnp.bfloat16).reshape(seq_count, kv_local, group_size, drafts, drafts),
        values_new,
        preferred_element_type=jnp.float32,
    )
    weighted = weighted.reshape(row_count, local_heads * head_dim)
    row_top = jnp.transpose(row_top, (0, 2, 1)).reshape(row_count, local_heads)
    row_total = jnp.transpose(row_total, (0, 2, 1)).reshape(row_count, local_heads)
    tops, totals, sums_rows = in_one_piece(
        (row_top[None], row_total[None], weighted[None]), "kv", 1, 0, 2
    )
    top_all = jnp.max(tops, axis=0)
    factors = jnp.exp(tops - top_all[None])
    total_all = jnp.sum(totals * factors, axis=0)
    share_rows = sums_rows.shape[1]
    merged = jnp.sum(
        sums_rows.reshape(-1, share_rows, local_heads, head_dim) * factors[..., None], axis=0
    )
    share = (
        (merged / total_all[..., None])
        .reshape(share_rows, local_heads * head_dim)
        .astype(jnp.bfloat16)
    )
    attended = collect(share, "kv", 0)
    partial_out = jnp.dot(attended, w_out, preferred_element_type=jnp.float32)
    mixed = gathered_total(partial_out.astype(jnp.bfloat16), "tp").astype(jnp.float32)
    return mixed.astype(jnp.bfloat16).reshape(seq_count, drafts, local_width)


def solution(mesh):
    return jax.shard_map(
        body,
        mesh=mesh,
        in_specs=(
            P(None, None, "kv"),
            P("kv"),
            P("kv", "tp"),
            P("kv", "tp"),
            P("kv", "tp"),
            P(),
            P("tp"),
            P(),
            P(),
            P("tp", "kv"),
            P(None, "tp", "kv"),
            P(None, "tp", "kv"),
            P(None, "tp", "kv"),
            P(),
            P(),
            P(),
        ),
        out_specs=P(None, None, "kv"),
        check_vma=False,
    )
```

profile of v0, /device:TPU:1, one launch (start us, length us, event | category | flops | bytes accessed | tf_op | source)
XLA Modules:
  0.0 219.7 jit_solution(5042115449655337162)
XLA Ops:
  6.5 0.7 convert_element_type.68
  7.2 1.3 multiply_reduce_fusion
  8.6 1.2 fusion.20
  9.9 0.4 fusion.47
  10.2 0.3 reshape.247
  10.6 0.9 broadcast_in_dim.43
  11.5 8.6 %all-to-all-start.1 = ((f32[16,1,5760]{2,1,0:T(1,128)}), f32[16,1,5760]{2,1,0:T(1,128)S(1)}, u32[]{:S(2)}, u32[]{:S(2)}) async-start(f32[16,1,5760]{2,1,0:T(1,128)} %broadcast_in_dim.43), calls=%async_computation.1 | async-start | bytes 737280 | tf_op jit(solution)/shard_map/all_to_all | solution.py:12
  20.2 0.8 convolution_minimum_fusion.4
  21.0 0.6 convolution_minimum_fusion.2
  21.6 0.1 copy.167
  21.7 0.1 copy.168
  21.9 1.5 convolution_convert_fusion
  23.3 5.7 %all-to-all-done.1 = f32[16,1,5760]{2,1,0:T(1,128)S(1)} async-done(((f32[16,1,5760]{2,1,0:T(1,128)}), f32[16,1,5760]{2,1,0:T(1,128)S(1)}, u32[]{:S(2)}, u32[]{:S(2)}) %all-to-all-start.1) | async-done | bytes 368672 | tf_op jit(solution)/shard_map/all_to_all | solution.py:12
  29.0 3.6 %all-to-all-start = ((bf16[16,72,384]{2,1,0:T(8,128)(2,1)}), bf16[16,72,384]{2,1,0:T(8,128)(2,1)S(1)}, u32[]{:S(2)}, u32[]{:S(2)}) async-start(bf16[16,72,384]{2,1,0:T(8,128)(2,1)} %bitcast.1), calls=%async_computation | async-start | bytes 1769472 | tf_op jit(solution)/shard_map/all_to_all | solution.py:38
  32.8 0.6 compare_and_fusion
  33.5 0.3 copy.175
  33.8 0.1 iota_compare_fusion.2
  33.9 0.2 reduce_sum.107
  34.2 12.0 %all-to-all-done = bf16[16,72,384]{2,1,0:T(8,128)(2,1)S(1)} async-done(((bf16[16,72,384]{2,1,0:T(8,128)(2,1)}), bf16[16,72,384]{2,1,0:T(8,128)(2,1)S(1)}, u32[]{:S(2)}, u32[]{:S(2)}) %all-to-all-start) | async-done | bytes 884768 | tf_op jit(solution)/shard_map/all_to_all | solution.py:38
  46.2 0.1 convert_reduce_fusion
  46.4 0.1 multiply_reduce_fusion.1
  46.7 0.1 mul.158
  46.8 0.1 reduce_sum.108
  47.0 0.1 mul.159
  47.1 0.1 mul.160
  47.4 1.0 broadcast_in_dim.45
  48.4 4.1 %all-to-all-start.2 = ((bf16[16,72,384]{2,1,0:T(8,128)(2,1)}), bf16[16,72,384]{2,1,0:T(8,128)(2,1)S(1)}, u32[]{:S(2)}, u32[]{:S(2)}) async-start(bf16[16,72,384]{2,1,0:T(8,128)(2,1)} %broadcast_in_dim.45), calls=%async_computation.2 | async-start | bytes 1769472 | tf_op jit(solution)/shard_map/all_to_all | solution.py:12
  52.5 0.2 all-gather.3.cloned.1.call-start
  52.8 0.4 select_reduce_fusion.4
  53.1 0.1 broadcast_compare_fusion
  53.4 0.6 reshape.251
  54.0 0.3 copy.178
  54.3 0.1 fusion.41
  54.4 0.1 copy.179
  54.5 0.3 fusion.61
  54.8 11.1 %all-to-all-done.2 = bf16[16,72,384]{2,1,0:T(8,128)(2,1)S(1)} async-done(((bf16[16,72,384]{2,1,0:T(8,128)(2,1)}), bf16[16,72,384]{2,1,0:T(8,128)(2,1)S(1)}, u32[]{:S(2)}, u32[]{:S(2)}) %all-to-all-start.2) | async-done | bytes 884768 | tf_op jit(solution)/shard_map/all_to_all | solution.py:12
  65.9 0.9 fusion.60
  66.9 1.5 reshape.249
  68.4 6.5 %select_reduce_fusion.1 = (f32[48,4,24]{2,1,0:T(4,128)S(1)}, f32[48,24,4,1024]{3,1,2,0:T(8,128)S(1)}) fusion(f32[48,4,1024]{2,1,0:T(4,128)} %param.28, pred[48,1024]{1,0:T(8,128)(4,1)S(1)} %broadcast_compare_fusion, bf16[48,64,1024]{2,1,0:T(8,128)(2,1)} %param.26, bf16[48,24,4,64]{3,2,1,0:T(4,128)(2,1)} %reshape.249), kind=kOutput, calls=%fused_computation.7 | convolution fusion | flops 622849536 | bytes 26609664 | tf_op jit(solution)/shard_map/oxfzu,ofuq->ofzxq/dot_general | solution.py:184
  74.9 4.6 %select_reduce_fusion.3 = (f32[48,4,24]{2,1,0:T(4,128)S(1)}, f32[48,24,24,4]{2,1,3,0:T(8,128)S(1)}) fusion(f32[48,4,24]{2,1,0:T(4,128)S(1)} %fusion.61, f32[48,4]{1,0:T(8,128)S(1)} %select_reduce_fusion.4, pred[48,24,24]{1,2,0:T(8,128)(4,1)S(1)} %copy.175, bf16[48,24,64,1]{2,1,3,0:T(8,128)(2,1)} %bitcast.131, bf16[48,24,4,64]{3,2,1,0:T(4,128)(2,1)} %reshape.249), kind=kOutput, calls=%fused_computation.27 | convolution fusion | flops 14704128 | bytes 1244928 | tf_op jit(solution)/shard_map/bpkgd,bjkd->bkgpj/dot_general | solution.py:188
  79.5 2.1 copy-done.3
  81.6 2.2 %select_reduce_fusion.2 = f32[48,4,24]{2,1,0:T(4,128)} fusion(f32[48,24,24,4]{2,1,3,0:T(8,128)S(1)} %get-tuple-element.17, f32[48,4,24]{2,1,0:T(4,128)S(1)} %max.24, f32[48,4,24]{2,1,0:T(4,128)S(1)} %fusion.61, f32[48,4]{1,0:T(8,128)S(1)} %select_reduce_fusion.4, pred[48,24,24]{1,2,0:T(8,128)(4,1)S(1)} %copy.175), kind=kLoop, calls=%fused_computation.26 | loop fusion | flops 658944 | bytes 526080 | tf_op jit(solution)/shard_map/reduce_sum | solution.py:202
  83.8 5.8 %select_reduce_fusion = f32[48,4,24]{2,1,0:T(4,128)S(1)} fusion(f32[48,24,4,1024]{3,1,2,0:T(8,128)S(1)} %get-tuple-element.13, f32[48,4,24]{2,1,0:T(4,128)S(1)} %max.24, f32[48,4,1024]{2,1,0:T(4,128)S(1)} %copy-done.6, pred[48,1024]{1,0:T(8,128)(4,1)S(1)} %broadcast_compare_fusion), kind=kLoop, calls=%fused_computation.6 | loop fusion | flops 23588352 | bytes 19746816 | tf_op jit(solution)/shard_map/reduce_sum | solution.py:202
  89.6 13.5 %fusion.5 = f32[48,4,24,64]{3,2,1,0:T(8,128)} fusion(f32[48,24,4,1024]{3,1,2,0:T(8,128)} %copy-done.2, f32[48,4,24]{2,1,0:T(4,128)S(1)} %max.24, f32[48,4,1024]{2,1,0:T(4,128)} %param.28, pred[48,1024]{1,0:T(8,128)(4,1)S(1)} %broadcast_compare_fusion, bf16[48,64,1024]{2,1,0:T(8,128)(2,1)} %param.27), kind=kOutput, calls=%fused_computation.9 | convolution fusion | flops 627572736 | bytes 27199488 | tf_op jit(solution)/shard_map/ftxwm,ftnm->fwtxn/dot_general | solution.py:203
  103.1 3.9 %fusion.16 = f32[48,24,1,4,64]{4,1,3,0,2:T(8,128)S(1)} fusion(f32[48,4,24,64]{3,2,1,0:T(8,128)} %fusion.5, bf16[48,24,64,1]{2,1,3,0:T(8,128)(2,1)S(1)} %bitcast.130, f32[48,24,24,4]{2,1,3,0:T(8,128)S(1)} %copy-done.4, f32[48,4,24]{2,1,0:T(4,128)S(1)} %max.24, f32[48,4,24]{2,1,0:T(4,128)S(1)} %fusion.61, f32[48,4]{1,0:T(8,128)S(1)} %select_reduce_fusion.4, ...), kind=kOutput, calls=%fused_computation.24 | convolution fusion | flops 15114240 | bytes 3014400 | tf_op jit(solution)/shard_map/bkgpj,bjkd->bpkgd/dot_general | solution.py:211
  107.0 0.6 copy.184
  107.6 2.3 %broadcast_in_dim_reshape.11 = f32[1,1152,256]{2,1,0:T(8,128)} reshape(f32[48,24,1,4,64]{4,3,1,0,2:T(4,128)S(1)} %copy.184) | data formatting | bytes 2359296 | tf_op jit(solution)/shard_map/broadcast_in_dim;reshape | solution.py:221
  109.9 0.4 copy.200
  110.3 0.4 copy.199
  110.7 0.5 copy-done.7
  111.2 0.8 pad_maximum_fusion
  112.0 13.3 %copy.187 = f32[1,1152,264]{2,0,1:T(1,128)S(1)} copy(f32[1,1152,264]{2,1,0:T(8,128)S(1)} %pad_maximum_fusion) | data formatting | bytes 2433024 | tf_op jit(solution)/shard_map/concatenate | solution.py:57
  125.3 25.5 %all_to_all.33 = f32[1,1152,264]{2,0,1:T(1,128)S(1)} all-to-all(f32[1,1152,264]{2,0,1:T(1,128)S(1)} %copy.187), channel_id=1, replica_groups=mesh['kv'=16,'tp'=8] {'kv'}, dimensions={1} | all-to-all | bytes 2433024 | tf_op jit(solution)/shard_map/all_to_all | solution.py:60
  150.8 3.8 %copy.188 = f32[1,1152,264]{1,2,0:T(8,128)} copy(f32[1,1152,264]{2,0,1:T(1,128)S(1)} %all_to_all.33) | data formatting | bytes 2433024 | tf_op jit(solution)/shard_map/all_to_all | solution.py:60
  154.6 3.0 %all_to_all.26 = f32[16,72,264]{1,0,2:T(8,128)S(1)} reshape(f32[1,1152,264]{1,2,0:T(8,128)} %copy.188) | data formatting | bytes 2433024 | tf_op jit(solution)/shard_map/all_to_all | solution.py:60
  157.6 0.1 fusion.42
  157.7 0.4 fusion.17
  158.3 0.1 copy.191
  158.4 0.1 div.39
  158.5 0.1 div.40
  158.7 12.6 %all_to_all.34 = bf16[16,72,256]{2,1,0:T(8,128)(2,1)S(1)} all-to-all(bf16[16,72,256]{2,1,0:T(8,128)(2,1)S(1)} %broadcast_in_dim.102), channel_id=1, replica_groups=mesh['kv'=16,'tp'=8] {'kv'}, dimensions={0} | all-to-all | bytes 1179648 | tf_op jit(solution)/shard_map/all_to_all | solution.py:12
  171.3 1.1 convolution_convert_fusion.1
  172.5 36.4 %all-gather.3.cloned.1.call-done = bf16[9216,256]{1,0:T(8,128)(2,1)} async-done(((bf16[1152,256]{1,0:T(8,128)(2,1)}), bf16[9216,256]{1,0:T(8,128)(2,1)}) %all-gather.3.cloned.1.call-update) | async-done | bytes 4718608 | tf_op jit(solution)/shard_map/all_gather | solution.py:68
  208.9 4.0 %reduce_sum.115 = bf16[1152,256]{1,0:T(8,128)(2,1)} reduce(bf16[8,1152,256]{2,1,0:T(8,128)(2,1)} %bitcast.125, bf16[]{:T(256)} %constant.59.clone.1), dimensions={0}, to_apply=%region_13.14 | reduce | flops 2064384 | bytes 5308418 | tf_op jit(solution)/shard_map/reduce_sum | solution.py:69
  (67 shorter events, 1.2 us)
Async XLA Ops:
  6.5 3.3 %copy-start = (bf16[4096,32]{0,1:T(8,128)(2,1)S(1)}, bf16[4096,32]{0,1:T(8,128)(2,1)}, u32[]{:S(2)}) copy-start(bf16[4096,32]{0,1:T(8,128)(2,1)} %param.21) | copy-start | bytes 786436
  7.2 12.9 %copy-start.14 = (s32[48,24]{0,1:T(8,128)S(1)}, s32[48,24]{0,1:T(8,128)}, u32[]{:S(2)}) copy-start(s32[48,24]{0,1:T(8,128)} %param.29) | copy-start | bytes 13828
  9.8 11.8 %copy-start.12 = (bf16[256,64]{0,1:T(8,128)(2,1)S(1)}, bf16[256,64]{0,1:T(8,128)(2,1)}, u32[]{:S(2)}) copy-start(bf16[256,64]{0,1:T(8,128)(2,1)} %param.19) | copy-start | bytes 98308
  9.8 11.9 %copy-start.13 = (bf16[256,64]{0,1:T(8,128)(2,1)S(1)}, bf16[256,64]{0,1:T(8,128)(2,1)}, u32[]{:S(2)}) copy-start(bf16[256,64]{0,1:T(8,128)(2,1)} %param.20) | copy-start | bytes 98308
  9.9 12.0 %copy-start.11 = (bf16[256,256]{1,0:T(8,128)(2,1)S(1)}, bf16[256,256]{1,0:T(8,128)(2,1)}, u32[]{:S(2)}) copy-start(bf16[256,256]{1,0:T(8,128)(2,1)} %param.18) | copy-start | bytes 393220
  11.5 17.6 %all-to-all-start.1 = ((f32[16,1,5760]{2,1,0:T(1,128)}), f32[16,1,5760]{2,1,0:T(1,128)S(1)}, u32[]{:S(2)}, u32[]{:S(2)}) async-start(f32[16,1,5760]{2,1,0:T(1,128)} %broadcast_in_dim.43), calls=%async_computation.1 | async-start | bytes 737280 | tf_op jit(solution)/shard_map/all_to_all | solution.py:12
  21.0 11.7 %copy-start.17 = (s32[48]{0:T(128)S(1)}, s32[48]{0:T(128)}, u32[]{:S(2)}) copy-start(s32[48]{0:T(128)} %param.30) | copy-start | bytes 580
  21.0 11.7 %copy-start.18 = (s32[48]{0:T(128)S(1)}, s32[48]{0:T(128)}, u32[]{:S(2)}) copy-start(s32[48]{0:T(128)} %param.31) | copy-start | bytes 580
  21.0 11.7 %copy-start.19 = (bf16[64]{0:T(256)(128)(2,1)S(1)}, bf16[64]{0:T(256)(128)(2,1)}, u32[]{:S(2)}) copy-start(bf16[64]{0:T(256)(128)(2,1)} %param.24) | copy-start | bytes 388
  21.0 11.8 %copy-start.16 = (bf16[64]{0:T(256)(128)(2,1)S(1)}, bf16[64]{0:T(256)(128)(2,1)}, u32[]{:S(2)}) copy-start(bf16[64]{0:T(256)(128)(2,1)} %param.23) | copy-start | bytes 388
  29.0 17.2 %all-to-all-start = ((bf16[16,72,384]{2,1,0:T(8,128)(2,1)}), bf16[16,72,384]{2,1,0:T(8,128)(2,1)S(1)}, u32[]{:S(2)}, u32[]{:S(2)}) async-start(bf16[16,72,384]{2,1,0:T(8,128)(2,1)} %bitcast.1), calls=%async_computation | async-start | bytes 1769472 | tf_op jit(solution)/shard_map/all_to_all | solution.py:38
  46.3 6.4 %copy-start.5 = (f32[48,4,1024]{2,1,0:T(4,128)S(1)}, f32[48,4,1024]{2,1,0:T(4,128)}, u32[]{:S(2)}) copy-start(f32[48,4,1024]{2,1,0:T(4,128)} %param.28) | copy-start | bytes 2359300
  47.4 6.9 %copy-start.15 = (f32[4]{0:T(128)S(1)}, f32[4]{0:T(128)}, u32[]{:S(2)}) copy-start(f32[4]{0:T(128)} %param.22) | copy-start | bytes 52
  48.4 17.5 %all-to-all-start.2 = ((bf16[16,72,384]{2,1,0:T(8,128)(2,1)}), bf16[16,72,384]{2,1,0:T(8,128)(2,1)S(1)}, u32[]{:S(2)}, u32[]{:S(2)}) async-start(bf16[16,72,384]{2,1,0:T(8,128)(2,1)} %broadcast_in_dim.45), calls=%async_computation.2 | async-start | bytes 1769472 | tf_op jit(solution)/shard_map/all_to_all | solution.py:12
  52.5 156.3 %all-gather.3.cloned.1.call-start = ((), (), s32[]{:S(2)}) async-start(), calls=%async_computation.5 | async-start | bytes 5308416 | tf_op jit(solution)/shard_map/all_gather | solution.py:68
  74.9 8.9 %copy-start.2 = (f32[48,24,4,1024]{3,1,2,0:T(8,128)}, f32[48,24,4,1024]{3,1,2,0:T(8,128)S(1)}, u32[]{:S(2)}) copy-start(f32[48,24,4,1024]{3,1,2,0:T(8,128)S(1)} %get-tuple-element.13) | copy-start | bytes 56623108
  79.4 2.1 copy-start.3
  79.5 4.3 %copy-start.6 = (f32[48,4,1024]{2,1,0:T(4,128)S(1)}, f32[48,4,1024]{2,1,0:T(4,128)}, u32[]{:S(2)}) copy-start(f32[48,4,1024]{2,1,0:T(4,128)} %param.28) | copy-start | bytes 2359300
  89.6 13.5 %copy-start.4 = (f32[48,24,24,4]{2,1,3,0:T(8,128)S(1)}, f32[48,24,24,4]{2,1,3,0:T(8,128)}, u32[]{:S(2)}) copy-start(f32[48,24,24,4]{2,1,3,0:T(8,128)} %copy-done.3) | copy-start | bytes 1327108
  89.6 13.5 %copy-start.8 = (bf16[1152,64]{1,0:T(8,128)(2,1)S(1)}, bf16[1152,64]{1,0:T(8,128)(2,1)}, u32[]{:S(2)}) copy-start(bf16[1152,64]{1,0:T(8,128)(2,1)} %get-tuple-element.10) | copy-start | bytes 442372
  107.6 2.3 %copy-start.9 = (f32[48,4,24]{2,1,0:T(4,128)S(1)}, f32[48,4,24]{2,1,0:T(4,128)}, u32[]{:S(2)}) copy-start(f32[48,4,24]{2,1,0:T(4,128)} %select_reduce_fusion.2) | copy-start | bytes 55300
  109.9 1.3 copy-start.7
  157.7 13.6 %copy-start.10 = (bf16[256,256]{1,0:T(8,128)(2,1)S(1)}, bf16[256,256]{1,0:T(8,128)(2,1)}, u32[]{:S(2)}) copy-start(bf16[256,256]{1,0:T(8,128)(2,1)} %param.25) | copy-start | bytes 393220
  208.9 4.0 %copy-start.1 = (bf16[4096,32]{0,1:T(8,128)(2,1)S(1)}, bf16[4096,32]{0,1:T(8,128)(2,1)}, u32[]{:S(2)}) copy-start(bf16[4096,32]{0,1:T(8,128)(2,1)} %param.21) | copy-start | bytes 786436
Sparse Core Ops, SparseCore 0:
  172.6 36.2 all-gather.2
where the time goes:
time: 220 us
  waiting for transfers between devices  65.2 us (30%)
  blocking collectives  38.1 us (17%)
  local copies, waits for them, and re-layouts  34.1 us (16%)
  matrix products  33.6 us (15%)
  other arithmetic  18.2 us (8%)
  starting transfers between devices  16.6 us (8%)
  between operations  14 us (6%)
    all_gather x1, waiting for transfers between devices, gathered_total(): tiles = lax.all_gather(shard, axis).astype(jnp.float32)  36.4 us
    all_to_all x1, blocking collectives, in_one_piece(): lax.all_to_all(both, axis, split_axis=split_dim, concat_axis=concat_dim,...  25.5 us
    all_to_all x2, waiting for transfers between devices, sent_to_all(): lax.all_to_all(jnp.broadcast_to(shard[None], (size, *shard.shape)), axis,...  16.8 us
    dot_general x1, matrix products, body(): jnp.einsum('ftxwm,ftnm->fwtxn', cache_weights.astype(jnp.bfloat16).reshap...  13.5 us
    concatenate x1, local copies, waits for them, and re-layouts, in_one_piece(): both = jnp.concatenate(arrays, axis=along)  13.3 us
    all_to_all x2, starting transfers between devices, sent_to_all(): lax.all_to_all(jnp.broadcast_to(shard[None], (size, *shard.shape)), axis,...  12.7 us
    all_to_all x1, blocking collectives, sent_to_all(): lax.all_to_all(jnp.broadcast_to(shard[None], (size, *shard.shape)), axis,...  12.6 us
    all_to_all x1, waiting for transfers between devices, summed_on_arrival(): tiles = lax.all_to_all(in_blocks(shard, dim, size), axis, 0, 0, tiled=True)  12 us
  transfers between devices with their start and end apart: 4, of which 4 were waited for; matrix products, arithmetic and copies ran while one was open for 3% of the time, Pallas kernels for 0%

commit v1 on v0

v1 whole, which is shorter than its diff:
```python
import functools

import jax
import jax.numpy as jnp
from jax import lax
from jax.experimental import pallas as pl
from jax.experimental.pallas import tpu as pltpu
from jax.sharding import PartitionSpec as P

f32, bf16 = jnp.float32, jnp.bfloat16
eps = 1e-05
floor_value = -1e30
KV_SIDE = 4
N_KV = 16
N_TP = 8
MESH = pl.DeviceIdType.MESH

PROJ, STAT, QUERY, PART, LSE, ATT, OUT, FINAL = range(8)


def dot(a, b):
    return jnp.dot(a, b, preferred_element_type=f32)


def dot_nt(a, b):
    return lax.dot_general(a, b, (((1,), (1,)), ((), ())), preferred_element_type=f32)


def halves(value):
    high = value.astype(bf16)
    return high, (value - high.astype(f32)).astype(bf16)


def padded(value, rows):
    return jnp.concatenate([value, jnp.zeros((rows - value.shape[0], value.shape[1]), value.dtype)], axis=0)


def lanes(shape):
    return lax.broadcasted_iota(jnp.int32, shape, 1)


def rows_of(shape):
    return lax.broadcasted_iota(jnp.int32, shape, 0)


def kernel(
    tokens, norm_gain, w_query, w_key, w_value, w_forget, forget_bias, query_gain, key_gain, w_out,
    key_cache, value_cache, gate_sums, parents, lengths, accepted,
    out,
    w_all, wf, keys, values, gates, reach, p_send, p_recv, s_send, s_recv, own_proj, q_all, kv_new,
    path_tile, o_send, o_recv, l_send, l_recv, a_all, t_send, t_recv, fin,
    local_sem, send_sem, recv_sem,
):
    kv = lax.axis_index("kv")
    tp = lax.axis_index("tp")
    z, y = kv // KV_SIDE, kv % KV_SIDE
    x, core = tp // 2, tp % 2
    share = q_all.shape[1]
    seqs = 3
    drafts = share // seqs
    heads = 4
    head_dim = 64
    width = heads * head_dim
    positions = key_cache.shape[2]
    model_width = w_forget.shape[0]

    def ahead(o):
        return ((z + o // KV_SIDE) % KV_SIDE) * KV_SIDE + (y + o % KV_SIDE) % KV_SIDE

    def behind(o):
        return ((z + KV_SIDE - o // KV_SIDE) % KV_SIDE) * KV_SIDE + (y + KV_SIDE - o % KV_SIDE) % KV_SIDE

    def tp_ahead(u):
        return ((x + u // 2) % 4) * 2 + (core + u) % 2

    def remote(kind, index, src, dst, device):
        return pltpu.make_async_remote_copy(
            src_ref=src, dst_ref=dst, send_sem=send_sem.at[kind, index], recv_sem=recv_sem.at[kind, index],
            device_id=device, device_id_type=MESH,
        )

    barrier = pltpu.get_barrier_semaphore()
    for o in range(1, N_KV):
        pl.semaphore_signal(barrier, inc=1, device_id={"kv": ahead(o)}, device_id_type=MESH)
    for u in range(1, N_TP):
        pl.semaphore_signal(barrier, inc=1, device_id={"tp": tp_ahead(u)}, device_id_type=MESH)

    wf_copy = pltpu.make_async_copy(w_forget.at[pl.ds(kv * 256, 256)], wf, local_sem.at[0])
    gate_copy = pltpu.make_async_copy(gate_sums, gates, local_sem.at[1])
    key_copy = pltpu.make_async_copy(key_cache, keys, local_sem.at[2])
    value_copy = pltpu.make_async_copy(value_cache, values, local_sem.at[3])
    wf_copy.start()
    gate_copy.start()
    key_copy.start()
    value_copy.start()

    w_all[:, :width] = w_query[...]
    w_all[:, width:] = jnp.concatenate([w_key[...].astype(f32), w_value[...].astype(f32)], axis=1).astype(bf16)
    wf_copy.wait()
    gate_copy.wait()
    pick = (lanes((8, 32)) == rows_of((8, 32)) + 4 * tp) & (rows_of((8, 32)) < 4)
    gate_weights = dot_nt(pick.astype(f32).astype(bf16), wf[...]).astype(bf16)
    square_row = (rows_of((8, 256)) == 4).astype(f32).astype(bf16)
    gain = norm_gain[...].astype(f32)
    place = lanes((heads, positions)) + kv * positions
    tile_lane = lanes((8, 128))
    tile_row = rows_of((8, 128))

    def project(o, carry):
        chunk = ahead(o)
        wide = padded(tokens[chunk].astype(f32), 128)
        scaled = (wide * gain).astype(bf16)
        high, low = halves(wide * wide)
        tile = dot_nt(gate_weights, scaled) + dot_nt(square_row, high) + dot_nt(square_row, low)
        for j in range(seqs):
            b = chunk * seqs + j
            last = jnp.sum(
                jnp.where(place == lengths[b] + accepted[b] - 1, gates[b], 0.0), axis=1, keepdims=True
            )
            last = jnp.concatenate([last, jnp.zeros((4, 1), f32)], axis=0)
            tile = jnp.where(tile_lane == share + j, last, tile)
        s_send[o] = tile
        projected = dot(scaled, w_all[...])[:share]
        p_send[o] = projected.astype(bf16)
        own_proj[...] = projected
        return carry

    lax.fori_loop(0, N_KV, lambda i, c: project(N_KV - 1 - i, c), 0)

    pl.semaphore_wait(barrier, N_KV + N_TP - 2)
    for o in range(1, N_KV):
        remote(STAT, o, s_send.at[o], s_recv.at[o], {"kv": ahead(o)}).start()
        remote(PROJ, o, p_send.at[o], p_recv.at[o], {"kv": ahead(o)}).start()

    row_lane = lanes((1, 128))
    for j in range(seqs):
        for p in range(drafts):
            parent = parents[kv * seqs + j, p]
            at = jnp.where(parent >= 0, parent + drafts * j, -1)
            i = drafts * j + p
            reach[i : i + 1, :] = ((row_lane == i) | (row_lane == at)).astype(f32)
    reach[share:, :] = jnp.zeros((128 - share, 128), f32)
    closure = reach[...]
    for _ in range(5):
        closure = jnp.minimum(dot(closure.astype(bf16), closure.astype(bf16)), 1.0)
    reach[...] = closure

    head_of = lax.broadcasted_iota(jnp.int32, (384, 384), 0) // head_dim
    head_at = lax.broadcasted_iota(jnp.int32, (384, 384), 1) // head_dim
    head_mean = jnp.where(head_of == head_at, 1.0 / head_dim, 0.0).astype(bf16)
    gains = jnp.concatenate([query_gain[...].astype(f32)] * 4 + [key_gain[...].astype(f32)] * 2, axis=1)

    def add_in(o, carry):
        total, stats = carry
        remote(STAT, o, s_send.at[o], s_recv.at[o], {"kv": ahead(o)}).wait_recv()
        remote(PROJ, o, p_send.at[o], p_recv.at[o], {"kv": ahead(o)}).wait_recv()
        return total + p_recv[o].astype(f32), stats + s_recv[o]

    total, stats = lax.fori_loop(1, N_KV, add_in, (own_proj[...], s_send[0]))
    inverse_tile = lax.rsqrt(stats / model_width + eps)
    inverse = jnp.concatenate([inverse_tile] * 16, axis=0).T[:share, 4:5]
    total = total * inverse
    high, low = halves(total * total)
    mean_sq = dot(high, head_mean) + dot(low, head_mean)
    normed = total * lax.rsqrt(mean_sq + eps) * gains
    q_all[0] = (normed[:, :width].astype(bf16).astype(f32) * head_dim ** (-0.5)).astype(bf16)
    for o in range(1, N_KV):
        remote(QUERY, o, q_all.at[0], q_all.at[o], {"kv": ahead(o)}).start()
    kv_new[...] = jnp.concatenate([normed[:, width : width + head_dim], total[:, width + head_dim :]], axis=1)

    bias = jnp.where(
        tile_row == 0, forget_bias[0],
        jnp.where(tile_row == 1, forget_bias[1], jnp.where(tile_row == 2, forget_bias[2], forget_bias[3])),
    )
    gate_pre = stats * inverse_tile[4:5, :] + bias
    log_gate = jnp.minimum(gate_pre, 0.0) - jnp.log1p(jnp.exp(-jnp.abs(gate_pre)))
    log_gate = jnp.where(tile_lane < share, log_gate, 0.0)
    top_part, rest = halves(log_gate)
    left = log_gate - top_part.astype(f32)
    middle, last_part = halves(left)
    follows = reach[...].astype(bf16)
    path = dot_nt(top_part, follows) + dot_nt(middle, follows) + dot_nt(last_part, follows)
    last_gate = jnp.where(
        tile_lane < drafts, stats[:, share : share + 1],
        jnp.where(tile_lane < 2 * drafts, stats[:, share + 1 : share + 2], stats[:, share + 2 : share + 3]),
    )
    path_tile[...] = path + last_gate

    key_copy.wait()
    value_copy.wait()
    wide_lane = lanes((heads * drafts, 128))

    def attend(o, carry):
        src = behind(o)

        @pl.when(o > 0)
        def _():
            remote(QUERY, o, q_all.at[0], q_all.at[o], {"kv": ahead(o)}).wait_recv()

        queries = q_all[o].astype(f32)
        pieces, sums = [], jnp.zeros((heads * drafts, 128), f32)
        for j in range(seqs):
            b = src * seqs + j
            block = queries[j * drafts : (j + 1) * drafts]
            stacked = jnp.concatenate(
                [block[:, h * head_dim : (h + 1) * head_dim] for h in range(heads)], axis=0
            ).astype(bf16)
            logits = dot(stacked, keys[b])
            kept = jnp.where(place < lengths[b] + accepted[b], -gates[b], floor_value)
            tops, weights, totals = [], [], []
            for h in range(heads):
                row = logits[h * drafts : (h + 1) * drafts] + kept[h : h + 1]
                top = jnp.max(row, axis=1, keepdims=True)
                weight = jnp.exp(row - top)
                tops.append(top)
                weights.append(weight)
                totals.append(jnp.sum(weight, axis=1, keepdims=True))
            weighted = dot_nt(jnp.concatenate(weights, axis=0).astype(bf16), values[b])
            all_total = jnp.concatenate(totals, axis=0)
            weighted = weighted / all_total
            sums = jnp.where(wide_lane == j, jnp.concatenate(tops, axis=0) + jnp.log(all_total), sums)
            pieces.append(
                jnp.concatenate([weighted[h * drafts : (h + 1) * drafts] for h in range(heads)], axis=1)
            )
        o_send[o] = jnp.concatenate(pieces, axis=0).astype(bf16)
        l_send[o] = padded(sums, 128).T[:8]

        @pl.when(o > 0)
        def _():
            remote(LSE, o, l_send.at[o], l_recv.at[o], {"kv": src}).start()
            remote(PART, o, o_send.at[o], o_recv.at[o], {"kv": src}).start()

        return carry

    lax.fori_loop(0, N_KV, attend, 0)

    q_own = padded(q_all[0].astype(f32), 128)
    new = padded(kv_new[...], 128)
    k_own = new[:, :head_dim].astype(bf16)
    v_own = new[:, head_dim:].astype(bf16)
    seen = reach[...] > 0.5
    bias_tile = path_tile[...]
    new_parts, new_sums = [], []
    for h in range(heads):
        logits = dot_nt(q_own[:, h * head_dim : (h + 1) * head_dim].astype(bf16), k_own)
        logits = jnp.where(seen, logits - bias_tile[h : h + 1, :], floor_value)
        top = jnp.max(logits, axis=1, keepdims=True)
        weight = jnp.where(seen, jnp.exp(logits - top), 0.0)
        total_new = jnp.sum(weight, axis=1, keepdims=True)
        new_parts.append((dot(weight.astype(bf16), v_own) / total_new)[:share])
        new_sums.append(top + jnp.log(total_new))
    new_part = jnp.concatenate(new_parts, axis=1)
    columns = jnp.zeros((heads * drafts, 128), f32)
    for j in range(seqs):
        column = jnp.concatenate([s[j * drafts : (j + 1) * drafts] for s in new_sums], axis=0)
        columns = jnp.where(wide_lane == j, column, columns)
    new_tile = padded(columns, 128).T[:8]

    tiles = [l_send[0]]
    for o in range(1, N_KV):
        remote(LSE, o, l_send.at[o], l_recv.at[o], {"kv": ahead(o)}).wait_recv()
        tiles.append(l_recv[o])
    tiles.append(new_tile)
    top_all = functools.reduce(jnp.maximum, tiles)
    factors = [jnp.exp(t - top_all) for t in tiles]
    whole = functools.reduce(jnp.add, factors)
    shares = [f / whole for f in factors]
    spread = jnp.concatenate(shares[:N_KV], axis=0).T
    spread_new = jnp.concatenate([shares[N_KV]] * 16, axis=0).T
    low_half = lanes((drafts, 128)) < head_dim

    def factor_rows(table, at):
        parts = []
        for j in range(seqs):
            column = table[:, at + j : at + j + 1]
            parts.append(
                jnp.concatenate(
                    [
                        jnp.where(
                            low_half,
                            column[2 * g * drafts : (2 * g + 1) * drafts],
                            column[(2 * g + 1) * drafts : (2 * g + 2) * drafts],
                        )
                        for g in range(2)
                    ],
                    axis=1,
                )
            )
        return jnp.concatenate(parts, axis=0)

    merged = new_part * factor_rows(spread_new, 0) + o_send[0].astype(f32) * factor_rows(spread, 0)
    for o in range(1, N_KV):
        remote(PART, o, o_send.at[o], o_recv.at[o], {"kv": ahead(o)}).wait_recv()
        merged = merged + o_recv[o].astype(f32) * factor_rows(spread, 8 * o)
    a_all[0] = merged.astype(bf16)
    for o in range(1, N_KV):
        remote(ATT, o, a_all.at[0], a_all.at[o], {"kv": ahead(o)}).start()

    def place_of(o):
        chunk = behind(o)
        owner, half = chunk // 2, chunk % 2
        u = ((owner // 2 + 4 - x) % 4) * 2 + (owner % 2 + 2 - core) % 2
        return owner, half, u

    def out_copy(o):
        owner, half, u = place_of(o)
        return remote(OUT, u * 2 + half, t_send.at[o], t_recv.at[u * 2 + half], {"tp": owner})

    def output(o, carry):
        @pl.when(o > 0)
        def _():
            remote(ATT, o, a_all.at[0], a_all.at[o], {"kv": ahead(o)}).wait_recv()

        part = dot(a_all[o], w_out[...]).astype(bf16)
        owner, half, u = place_of(o)
        t_send[o] = part

        @pl.when(u == 0)
        def _():
            t_recv[half] = part

        @pl.when(u != 0)
        def _():
            out_copy(o).start()

        return carry

    lax.fori_loop(0, N_KV, output, 0)
    for half in range(2):
        summed = t_recv[half].astype(f32)
        for u in range(1, N_TP):
            at = u * 2 + half
            remote(OUT, at, t_send.at[0], t_recv.at[at], {"tp": tp_ahead(u)}).wait_recv()
            summed = summed + t_recv[at].astype(f32)
        fin[half] = summed.astype(bf16)
        out[tp * 2 + half] = summed.astype(bf16)
        for u in range(1, N_TP):
            remote(FINAL, u * 2 + half, fin.at[half], out.at[tp * 2 + half], {"tp": tp_ahead(u)}).start()
    for half in range(2):
        for u in range(1, N_TP):
            copy = remote(FINAL, u * 2 + half, fin.at[half], out.at[tp * 2 + half], {"tp": tp_ahead(u)})
            copy.wait_recv()
            copy.wait_send()
            remote(OUT, u * 2 + half, t_send.at[0], t_recv.at[u * 2 + half], {"tp": tp_ahead(u)}).wait_send()
    for o in range(1, N_KV):
        device = {"kv": ahead(o)}
        remote(STAT, o, s_send.at[o], s_recv.at[o], device).wait_send()
        remote(PROJ, o, p_send.at[o], p_recv.at[o], device).wait_send()
        remote(QUERY, o, q_all.at[0], q_all.at[o], device).wait_send()
        remote(LSE, o, l_send.at[o], l_recv.at[o], device).wait_send()
        remote(PART, o, o_send.at[o], o_recv.at[o], device).wait_send()
        remote(ATT, o, a_all.at[0], a_all.at[o], device).wait_send()


def body(
    tokens, norm_gain, w_query, w_key, w_value, w_forget, forget_bias, query_gain, key_gain, w_out,
    key_cache, value_cache, gate_sums, parents, lengths, accepted,
):
    seq_count, drafts, local_width = tokens.shape
    share = seq_count * drafts // N_KV
    vmem = pl.BlockSpec(memory_space=pltpu.VMEM)
    smem = pl.BlockSpec(memory_space=pltpu.SMEM)
    anywhere = pl.BlockSpec(memory_space=pl.ANY)
    mixed = pl.pallas_call(
        kernel,
        out_shape=jax.ShapeDtypeStruct((N_KV, share, local_width), bf16),
        in_specs=[
            vmem, vmem, vmem, vmem, vmem, anywhere, smem, vmem, vmem, vmem,
            anywhere, anywhere, anywhere, smem, smem, smem,
        ],
        out_specs=vmem,
        scratch_shapes=[
            pltpu.VMEM((local_width, 384), bf16),
            pltpu.VMEM((local_width, w_forget.shape[1]), bf16),
            pltpu.VMEM(key_cache.shape, bf16),
            pltpu.VMEM(value_cache.shape, bf16),
            pltpu.VMEM(gate_sums.shape, f32),
            pltpu.VMEM((128, 128), f32),
            pltpu.VMEM((N_KV, share, 384), bf16),
            pltpu.VMEM((N_KV, share, 384), bf16),
            pltpu.VMEM((N_KV, 8, 128), f32),
            pltpu.VMEM((N_KV, 8, 128), f32),
            pltpu.VMEM((share, 384), f32),
            pltpu.VMEM((N_KV, share, 256), bf16),
            pltpu.VMEM((share, 128), f32),
            pltpu.VMEM((8, 128), f32),
            pltpu.VMEM((N_KV, share, 256), bf16),
            pltpu.VMEM((N_KV, share, 256), bf16),
            pltpu.VMEM((N_KV, 8, 128), f32),
            pltpu.VMEM((N_KV, 8, 128), f32),
            pltpu.VMEM((N_KV, share, 256), bf16),
            pltpu.VMEM((N_KV, share, 256), bf16),
            pltpu.VMEM((N_KV, share, 256), bf16),
            pltpu.VMEM((2, share, 256), bf16),
            pltpu.SemaphoreType.DMA((4,)),
            pltpu.SemaphoreType.DMA((8, 16)),
            pltpu.SemaphoreType.DMA((8, 16)),
        ],
        compiler_params=pltpu.CompilerParams(
            collective_id=0, has_side_effects=True, vmem_limit_bytes=56 * 1024 * 1024
        ),
        name="tree_attention",
    )(
        tokens.reshape(N_KV, share, local_width), norm_gain.reshape(1, -1), w_query, w_key, w_value, w_forget,
        forget_bias, query_gain.reshape(1, -1), key_gain.reshape(1, -1), w_out,
        key_cache, value_cache, gate_sums, parents, lengths, accepted,
    )
    return mixed.reshape(seq_count, drafts, local_width)


def solution(mesh):
    return jax.shard_map(
        body,
        mesh=mesh,
        in_specs=(
            P(None, None, "kv"),
            P("kv"),
            P("kv", "tp"),
            P("kv", "tp"),
            P("kv", "tp"),
            P(),
            P("tp"),
            P(),
            P(),
            P("tp", "kv"),
            P(None, "tp", "kv"),
            P(None, "tp", "kv"),
            P(None, "tp", "kv"),
            P(),
            P(),
            P(),
        ),
        out_specs=P(None, None, "kv"),
        check_vma=False,
    )
```

time: 220 us -> 89.5 us (0.41)
  Pallas kernels: 0 us -> 79.3 us
  waiting for transfers between devices: 65.2 us -> 0 us
  blocking collectives: 38.1 us -> 0 us
  matrix products: 33.6 us -> 0 us
  local copies, waits for them, and re-layouts: 34.1 us -> 9.8 us
  other arithmetic: 18.2 us -> 0 us
  starting transfers between devices: 16.6 us -> 0 us
  between operations: 14 us -> 0.01 us
    pallas_call x0 -> x1, Pallas kernels: none -> 79.3 us  [body(): pl.pallas_call(kernel, out_shape=jax.ShapeDtypeStruct((N_KV, share, local...]
    all_to_all x2 -> x0, blocking collectives: 38.1 us -> none  [the longest x1 25.5 us: in_one_piece(): lax.all_to_all(both, axis, split_axis=split_dim, concat_axis=concat_dim,...]
    all_gather x1 -> x0, waiting for transfers between devices: 36.4 us -> none  [gathered_total(): tiles = lax.all_gather(shard, axis).astype(jnp.float32)]
    dot_general x11 -> x0, matrix products: 33.6 us -> none  [the longest x1 13.5 us: body(): jnp.einsum('ftxwm,ftnm->fwtxn', cache_weights.astype(jnp.bfloat16).reshap...]
    all_to_all x3 -> x0, waiting for transfers between devices: 28.8 us -> none  [the longest x2 16.8 us: sent_to_all(): lax.all_to_all(jnp.broadcast_to(shard[None], (size, *shard.shape)), axis,...]
    all_to_all x3 -> x0, starting transfers between devices: 16.3 us -> none  [the longest x2 12.7 us: sent_to_all(): lax.all_to_all(jnp.broadcast_to(shard[None], (size, *shard.shape)), axis,...]
    reduce_sum x10 -> x0, other arithmetic: 14.6 us -> none  [the longest x2 7.98 us: body(): row_total = jnp.sum(cache_weights, axis=3) + jnp.sum(new_weights, axis=3)]
    concatenate x1 -> x0, local copies, waits for them, and re-layouts: 13.3 us -> none  [in_one_piece(): both = jnp.concatenate(arrays, axis=along)]
  transfers between devices with their start and end apart: 4 -> 0, of which waited for: 4 -> 0; matrix products, arithmetic and copies ran while one was open for 3% -> 0% of each run, Pallas kernels for 0% -> 0%
where the time goes in v1:
time: 89.5 us; the launch traced here: 89.1 us
  Pallas kernels  79.3 us (89%)
  local copies, waits for them, and re-layouts  9.8 us (11%)
    pallas_call x1, Pallas kernels, body(): pl.pallas_call(kernel, out_shape=jax.ShapeDtypeStruct((N_KV, share, local...  79.3 us
    unnamed x5, local copies, waits for them, and re-layouts  8.55 us

profile of v1, /device:TPU:1, one launch (start us, length us, event | category | flops | bytes accessed | tf_op | source)
XLA Modules:
  0.0 89.1 jit_solution(8687664778747298149)
XLA Ops:
  0.0 1.2 %reshape.16.norm_gain = bf16[1,256]{1,0:T(2,128)(2,1)} reshape(bf16[256]{0:T(256)(128)(2,1)} %param.17) | data formatting | bytes 1024 | tf_op jit(solution)/shard_map/reshape | solution.py:404
  1.3 1.4 %copy.20.parents = s32[48,24]{1,0:T(8,128)} copy(s32[48,24]{0,1:T(8,128)} %param.29) | data formatting | bytes 9216 | tf_op args[13]
  2.6 1.5 %copy.17.w_key = bf16[256,64]{1,0:T(8,128)(2,1)} copy(bf16[256,64]{0,1:T(8,128)(2,1)} %param.19) | data formatting | bytes 65536 | tf_op args[3]
  4.1 1.5 %copy.18.w_value = bf16[256,64]{1,0:T(8,128)(2,1)} copy(bf16[256,64]{0,1:T(8,128)(2,1)} %param.20) | data formatting | bytes 65536 | tf_op args[4]
  5.6 2.3 %copy.19.w_forget = bf16[4096,32]{1,0:T(8,128)(2,1)} copy(bf16[4096,32]{0,1:T(8,128)(2,1)} %param.21) | data formatting | bytes 524288 | tf_op args[5]
  7.9 79.3 %tree_attention.1 = bf16[16,72,256]{2,1,0:T(8,128)(2,1)} custom-call(bf16[16,72,256]{2,1,0:T(8,128)(2,1)} %bitcast.5, bf16[1,256]{1,0:T(2,128)(2,1)} %reshape.16.norm_gain, bf16[256,256]{1,0:T(8,128)(2,1)} %w_query.1, bf16[256,64]{1,0:T(8,128)(2,1)} %copy.17.w_key, bf16[256,64]{1,0:T(8,128)(2,1)} %copy.18.w_value, bf16[4096,32]{1,0:T(8,128)(2,1)} %copy.19.w_forget, ...), custom_call_target="tpu_custom_call" | custom-call | tf_op jit(solution)/shard_map/tree_attention/pallas_call | solution.py:364
  87.1 1.9 %copy.22 = bf16[48,24,256]{2,1,0:T(8,128)(2,1)} copy(bf16[48,24,256]{2,1,0:T(8,128)(2,1)} %bitcast.4) | data formatting | bytes 1179648

commit v2 on v1

v2 whole, which is shorter than its diff:
```python
import functools

import jax
import jax.numpy as jnp
from jax import lax
from jax.experimental import pallas as pl
from jax.experimental.pallas import tpu as pltpu
from jax.sharding import PartitionSpec as P

f32, bf16 = jnp.float32, jnp.bfloat16
eps = 1e-05
floor_value = -1e30
KV_SIDE = 4
N_KV = 16
N_TP = 8
MESH = pl.DeviceIdType.MESH

PROJ, STAT, QUERY, PART, LSE, ATT, OUT, FINAL = range(8)


def dot(a, b):
    return jnp.dot(a, b, preferred_element_type=f32)


def dot_nt(a, b):
    return lax.dot_general(a, b, (((1,), (1,)), ((), ())), preferred_element_type=f32)


def halves(value):
    high = value.astype(bf16)
    return high, (value - high.astype(f32)).astype(bf16)


def padded(value, rows):
    return jnp.concatenate([value, jnp.zeros((rows - value.shape[0], value.shape[1]), value.dtype)], axis=0)


def lanes(shape):
    return lax.broadcasted_iota(jnp.int32, shape, 1)


def rows_of(shape):
    return lax.broadcasted_iota(jnp.int32, shape, 0)


def kernel(
    tokens, norm_gain, w_query, w_key, w_value, w_forget, forget_bias, query_gain, key_gain, w_out,
    key_cache, value_cache, gate_sums, parents, lengths, accepted,
    out,
    w_kv, wf, keys, values, gates, reach, p_send, p_recv, s_send, s_recv, own_proj, q_all, q_own, kv_own,
    new_out, new_tile, o_send, o_recv, l_send, l_recv, a_all, t_send, t_recv, fin,
    local_sem, send_sem, recv_sem,
):
    kv = lax.axis_index("kv")
    tp = lax.axis_index("tp")
    z, y = kv // KV_SIDE, kv % KV_SIDE
    x, core = tp // 2, tp % 2
    seqs = 3
    drafts = tokens.shape[1]
    share = seqs * drafts
    heads = 4
    head_dim = 64
    width = heads * head_dim
    positions = key_cache.shape[2]
    model_width = w_forget.shape[1]

    def ahead(o):
        return ((z + o // KV_SIDE) % KV_SIDE) * KV_SIDE + (y + o % KV_SIDE) % KV_SIDE

    def behind(o):
        return ((z + KV_SIDE - o // KV_SIDE) % KV_SIDE) * KV_SIDE + (y + KV_SIDE - o % KV_SIDE) % KV_SIDE

    def tp_ahead(u):
        return ((x + u // 2) % 4) * 2 + (core + u) % 2

    def remote(kind, j, src, dst, device):
        return pltpu.make_async_remote_copy(
            src_ref=src, dst_ref=dst, send_sem=send_sem.at[kind, j], recv_sem=recv_sem.at[kind, j],
            device_id=device, device_id_type=MESH,
        )

    def arrived(kind, j, ref):
        remote(kind, j, ref, ref, {"kv": ahead(1)}).wait_recv()

    def gone(kind, j, ref):
        remote(kind, j, ref, ref, {"kv": ahead(1)}).wait_send()

    def others(ref, j):
        return ref.at[pl.ds(j * N_KV + 1, N_KV - 1)]

    barrier = pltpu.get_barrier_semaphore()
    for o in range(1, N_KV):
        pl.semaphore_signal(barrier, inc=1, device_id={"kv": ahead(o)}, device_id_type=MESH)
    for u in range(1, N_TP):
        pl.semaphore_signal(barrier, inc=1, device_id={"tp": tp_ahead(u)}, device_id_type=MESH)

    wf_copy = pltpu.make_async_copy(w_forget.at[:, pl.ds(kv * 256, 256)], wf, local_sem.at[0])
    gate_copy = pltpu.make_async_copy(gate_sums, gates, local_sem.at[1])
    key_copy = pltpu.make_async_copy(key_cache, keys, local_sem.at[2])
    value_copy = pltpu.make_async_copy(value_cache, values.at[:, pl.ds(0, head_dim)], local_sem.at[3])
    wf_copy.start()
    gate_copy.start()
    key_copy.start()
    value_copy.start()

    w_kv[...] = jnp.concatenate([w_key[...].astype(f32), w_value[...].astype(f32)], axis=0).astype(bf16)
    wf_copy.wait()
    gate_copy.wait()
    pick = (lanes((8, 32)) == rows_of((8, 32)) + 4 * tp) & (rows_of((8, 32)) < 4)
    gate_weights = dot(pick.astype(f32).astype(bf16), wf[...]).astype(bf16)
    square_row = (rows_of((8, 256)) == 4).astype(f32).astype(bf16)
    gain = norm_gain[...].astype(f32)
    gain = jnp.concatenate([gain[0:1], gain[1:2]], axis=1)
    place = lanes((heads, positions)) + kv * positions
    tile_lane = lanes((8, 128))
    tile_row = rows_of((8, 128))

    def project(o, carry):
        chunk = ahead(o)
        wide = jnp.concatenate([tokens[chunk * seqs + j].astype(f32) for j in range(seqs)], axis=0)
        wide = padded(wide, 128)
        scaled = (wide * gain).astype(bf16)
        high, low = halves(wide * wide)
        tile = dot_nt(gate_weights, scaled) + dot_nt(square_row, high) + dot_nt(square_row, low)
        for j in range(seqs):
            b = chunk * seqs + j
            last = jnp.sum(
                jnp.where(place == lengths[b] + accepted[b] - 1, gates[b], 0.0), axis=1, keepdims=True
            )
            last = jnp.concatenate([last, jnp.zeros((4, 1), f32)], axis=0)
            tile = jnp.where(tile_lane == share + j, last, tile)
        s_send[o] = tile
        projected = jnp.concatenate([dot(scaled, w_query[...]), dot_nt(scaled, w_kv[...])], axis=1)
        for j in range(seqs):
            p_send[j * N_KV + o] = projected[j * drafts : (j + 1) * drafts].astype(bf16)
        own_proj[...] = projected[:share]
        return carry

    lax.fori_loop(0, N_KV, lambda i, c: project(N_KV - 1 - i, c), 0)

    pl.semaphore_wait(barrier, N_KV + N_TP - 2)
    for o in range(1, N_KV):
        remote(STAT, 0, s_send.at[o], s_recv.at[o], {"kv": ahead(o)}).start()
    for j in range(seqs):
        for o in range(1, N_KV):
            at = j * N_KV + o
            remote(PROJ, j, p_send.at[at], p_recv.at[at], {"kv": ahead(o)}).start()

    row_lane = lanes((1, 128))
    for j in range(seqs):
        for p in range(drafts):
            parent = parents[p, kv * seqs + j]
            at = jnp.where(parent >= 0, parent + drafts * j, -1)
            i = drafts * j + p
            reach[i : i + 1, :] = ((row_lane == i) | (row_lane == at)).astype(f32)
    reach[share:, :] = jnp.zeros((128 - share, 128), f32)
    closure = reach[...]
    for _ in range(5):
        closure = jnp.minimum(dot(closure.astype(bf16), closure.astype(bf16)), 1.0)
    reach[...] = closure

    def set_ones(b, carry):
        values[b, head_dim:, :] = jnp.ones((16, positions), bf16)
        return carry

    lax.fori_loop(0, values.shape[0], set_ones, 0)

    head_of = lax.broadcasted_iota(jnp.int32, (384, 384), 0) // head_dim
    head_at = lax.broadcasted_iota(jnp.int32, (384, 384), 1) // head_dim
    head_mean = jnp.where(head_of == head_at, 1.0 / head_dim, 0.0).astype(bf16)
    gains = jnp.concatenate([query_gain[...].astype(f32)] * 4 + [key_gain[...].astype(f32)] * 2, axis=1)
    q_own[share:, :] = jnp.zeros((128 - share, width), f32)
    kv_own[share:, :] = jnp.zeros((128 - share, 128), f32)

    arrived(STAT, 0, others(s_recv, 0))
    stats = s_send[0]
    for o in range(1, N_KV):
        stats = stats + s_recv[o]
    inverse_tile = lax.rsqrt(stats / model_width + eps)
    inverse = jnp.concatenate([inverse_tile] * 16, axis=0).T
    for j in range(seqs):
        rows = slice(j * drafts, (j + 1) * drafts)
        arrived(PROJ, j, others(p_recv, j))
        total = own_proj[rows, :]
        for o in range(1, N_KV):
            total = total + p_recv[j * N_KV + o].astype(f32)
        total = total * inverse[rows, 4:5]
        high, low = halves(total * total)
        mean_sq = dot(high, head_mean) + dot(low, head_mean)
        normed = total * lax.rsqrt(mean_sq + eps) * gains
        query = normed[:, :width].astype(bf16).astype(f32) * head_dim ** (-0.5)
        q_all[j * N_KV] = query.astype(bf16)
        for o in range(1, N_KV):
            remote(QUERY, j, q_all.at[j * N_KV], q_all.at[j * N_KV + o], {"kv": ahead(o)}).start()
        q_own[rows, :] = query
        kv_own[rows, :] = jnp.concatenate(
            [normed[:, width : width + head_dim], total[:, width + head_dim :]], axis=1
        )

    bias = jnp.where(
        tile_row == 0, forget_bias[0],
        jnp.where(tile_row == 1, forget_bias[1], jnp.where(tile_row == 2, forget_bias[2], forget_bias[3])),
    )
    gate_pre = stats * inverse_tile[4:5, :] + bias
    log_gate = jnp.minimum(gate_pre, 0.0) - jnp.log1p(jnp.exp(-jnp.abs(gate_pre)))
    log_gate = jnp.where(tile_lane < share, log_gate, 0.0)
    top_part = log_gate.astype(bf16)
    middle, last_part = halves(log_gate - top_part.astype(f32))
    follows = reach[...].astype(bf16)
    path = dot_nt(top_part, follows) + dot_nt(middle, follows) + dot_nt(last_part, follows)
    last_gate = jnp.where(
        tile_lane < drafts, stats[:, share : share + 1],
        jnp.where(tile_lane < 2 * drafts, stats[:, share + 1 : share + 2], stats[:, share + 2 : share + 3]),
    )
    bias_tile = path + last_gate

    wide_lane = lanes((heads * drafts, 128))
    own_queries = q_own[...]
    k_own = kv_own[:, :head_dim].astype(bf16)
    v_own = kv_own[:, head_dim:].astype(bf16)
    seen = reach[...] > 0.5
    new_parts, new_sums = [], []
    for h in range(heads):
        logits = dot_nt(own_queries[:, h * head_dim : (h + 1) * head_dim].astype(bf16), k_own)
        logits = jnp.where(seen, logits - bias_tile[h : h + 1, :], floor_value)
        top = jnp.max(logits, axis=1, keepdims=True)
        weight = jnp.where(seen, jnp.exp(logits - top), 0.0)
        total_new = jnp.sum(weight, axis=1, keepdims=True)
        new_parts.append((dot(weight.astype(bf16), v_own) / total_new)[:share])
        new_sums.append(top + jnp.log(total_new))
    new_out[...] = jnp.concatenate(new_parts, axis=1)
    columns = jnp.zeros((heads * drafts, 128), f32)
    for j in range(seqs):
        column = jnp.concatenate([s[j * drafts : (j + 1) * drafts] for s in new_sums], axis=0)
        columns = jnp.where(wide_lane == j, column, columns)
    new_tile[...] = padded(columns, 128).T[:8]

    key_copy.wait()
    value_copy.wait()

    def attend(j, o, sums):
        src = behind(o)
        b = src * seqs + j
        at = j * N_KV + o
        block = q_all[at].astype(f32)
        stacked = jnp.concatenate(
            [block[:, h * head_dim : (h + 1) * head_dim] for h in range(heads)], axis=0
        ).astype(bf16)
        logits = dot(stacked, keys[b])
        kept = jnp.where(place < lengths[b] + accepted[b], -gates[b], floor_value)
        tops, weights = [], []
        for h in range(heads):
            row = logits[h * drafts : (h + 1) * drafts] + kept[h : h + 1]
            top = jnp.max(row, axis=1, keepdims=True)
            tops.append(top)
            weights.append(jnp.exp(row - top))
        weighted = dot_nt(jnp.concatenate(weights, axis=0).astype(bf16), values[b])
        total = weighted[:, head_dim : head_dim + 1]
        weighted = weighted[:, :head_dim] / total
        o_send[at] = jnp.concatenate(
            [weighted[h * drafts : (h + 1) * drafts] for h in range(heads)], axis=1
        ).astype(bf16)
        if o > 0:
            remote(PART, j, o_send.at[at], o_recv.at[at], {"kv": src}).start()
        return jnp.where(wide_lane == o, jnp.concatenate(tops, axis=0) + jnp.log(total), sums)

    def attend_all(j, first, last, sums):
        for o in range(first, last):
            if o == 1:
                arrived(QUERY, j, others(q_all, j))
            sums = attend(j, o, sums)
        if last < N_KV:
            return sums
        table = padded(sums, 128).T
        l_recv[j * N_KV] = table[:1]
        for o in range(1, N_KV):
            at = j * N_KV + o
            l_send[at] = table[o : o + 1]
        for o in range(1, N_KV):
            at = j * N_KV + o
            remote(LSE, j, l_send.at[at], l_recv.at[at], {"kv": behind(o)}).start()
        return sums

    low_half = lanes((drafts, 128)) < head_dim

    def merge(j):
        arrived(LSE, j, others(l_recv, j))
        table = jnp.concatenate([l_recv[j * N_KV + o] for o in range(N_KV)], axis=0)
        new = new_tile[j : j + 1, :]
        top = jnp.maximum(jnp.max(table, axis=0, keepdims=True), new)
        factors = jnp.exp(table - top)
        factor_new = jnp.exp(new - top)
        whole = jnp.sum(factors, axis=0, keepdims=True) + factor_new
        spread = padded(jnp.concatenate([factors / whole, padded(factor_new / whole, 8)], axis=0), 128).T

        def factor_rows(at):
            column = spread[:, at : at + 1]
            return jnp.concatenate(
                [
                    jnp.where(
                        low_half,
                        column[2 * g * drafts : (2 * g + 1) * drafts],
                        column[(2 * g + 1) * drafts : (2 * g + 2) * drafts],
                    )
                    for g in range(2)
                ],
                axis=1,
            )

        merged = new_out[j * drafts : (j + 1) * drafts, :] * factor_rows(N_KV)
        merged = merged + o_send[j * N_KV].astype(f32) * factor_rows(0)
        arrived(PART, j, others(o_recv, j))
        for o in range(1, N_KV):
            merged = merged + o_recv[j * N_KV + o].astype(f32) * factor_rows(o)
        a_all[j * N_KV] = merged.astype(bf16)
        for o in range(1, N_KV):
            remote(ATT, j, a_all.at[j * N_KV], a_all.at[j * N_KV + o], {"kv": ahead(o)}).start()

    def output(j):
        arrived(ATT, j, others(a_all, j))
        rows = jnp.concatenate([a_all[j * N_KV + o].astype(f32) for o in range(N_KV)], axis=0).astype(bf16)
        part = dot(rows, w_out[...])
        for o in range(N_KV):
            t_send[j * N_KV + o] = part[o * drafts : (o + 1) * drafts].astype(bf16)
        for u in range(N_TP):
            owner = tp_ahead(u)
            for half in range(2):
                chunk = owner * 2 + half
                o = ((z + 4 - chunk // 4) % 4) * 4 + (y + 4 - chunk % 4) % 4
                at = j * N_KV + u * 2 + half
                if u == 0:
                    t_recv[at] = t_send[j * N_KV + o]
                else:
                    remote(OUT, j, t_send.at[j * N_KV + o], t_recv.at[at], {"tp": owner}).start()

    def add_up(j):
        arrived(OUT, j, t_recv.at[pl.ds(j * N_KV + 2, N_KV - 2)])
        for half in range(2):
            summed = t_recv[j * N_KV + half].astype(f32)
            for u in range(1, N_TP):
                summed = summed + t_recv[j * N_KV + u * 2 + half].astype(f32)
            seq = (tp * 2 + half) * seqs + j
            fin[j * 2 + half] = summed.astype(bf16)
            out[seq] = summed.astype(bf16)
            for u in range(1, N_TP):
                remote(FINAL, j, fin.at[j * 2 + half], out.at[seq], {"tp": tp_ahead(u)}).start()

    none = jnp.zeros((heads * drafts, 128), f32)
    attend_all(0, 0, N_KV, none)
    attend_all(1, 0, N_KV, none)
    merge(0)
    sums = attend_all(2, 0, 10, none)
    merge(1)
    attend_all(2, 10, N_KV, sums)
    output(0)
    merge(2)
    output(1)
    add_up(0)
    add_up(1)
    output(2)
    add_up(2)
    for j in range(seqs):
        arrived(FINAL, j, t_recv.at[pl.ds(j * N_KV + 2, N_KV - 2)])
    gone(STAT, 0, others(s_send, 0))
    for j in range(seqs):
        gone(PROJ, j, others(p_send, j))
        gone(QUERY, j, others(q_all, j))
        gone(PART, j, others(o_send, j))
        gone(LSE, j, others(l_send, j))
        gone(ATT, j, others(a_all, j))
        gone(OUT, j, t_send.at[pl.ds(j * N_KV + 2, N_KV - 2)])
        gone(FINAL, j, t_send.at[pl.ds(j * N_KV + 2, N_KV - 2)])


def body(
    tokens, norm_gain, w_query, w_key, w_value, w_forget, forget_bias, query_gain, key_gain, w_out,
    key_cache, value_cache, gate_sums, parents, lengths, accepted,
):
    seq_count, drafts, local_width = tokens.shape
    share = seq_count * drafts // N_KV
    vmem = pl.BlockSpec(memory_space=pltpu.VMEM)
    smem = pl.BlockSpec(memory_space=pltpu.SMEM)
    anywhere = pl.BlockSpec(memory_space=pl.ANY)
    mixed = pl.pallas_call(
        kernel,
        out_shape=jax.ShapeDtypeStruct(tokens.shape, bf16),
        in_specs=[
            vmem, vmem, vmem, vmem, vmem, anywhere, smem, vmem, vmem, vmem,
            anywhere, anywhere, anywhere, smem, smem, smem,
        ],
        out_specs=vmem,
        scratch_shapes=[
            pltpu.VMEM((128, local_width), bf16),
            pltpu.VMEM((w_forget.shape[1], local_width), bf16),
            pltpu.VMEM(key_cache.shape, bf16),
            pltpu.VMEM((seq_count, value_cache.shape[1] + 16, value_cache.shape[2]), bf16),
            pltpu.VMEM(gate_sums.shape, f32),
            pltpu.VMEM((128, 128), f32),
            pltpu.VMEM((seq_count, drafts, 384), bf16),
            pltpu.VMEM((seq_count, drafts, 384), bf16),
            pltpu.VMEM((N_KV, 8, 128), f32),
            pltpu.VMEM((N_KV, 8, 128), f32),
            pltpu.VMEM((share, 384), f32),
            pltpu.VMEM((seq_count, drafts, 256), bf16),
            pltpu.VMEM((128, 256), f32),
            pltpu.VMEM((128, 128), f32),
            pltpu.VMEM((share, 256), f32),
            pltpu.VMEM((8, 128), f32),
            pltpu.VMEM((seq_count, drafts, 256), bf16),
            pltpu.VMEM((seq_count, drafts, 256), bf16),
            pltpu.VMEM((seq_count, 1, 128), f32),
            pltpu.VMEM((seq_count, 1, 128), f32),
            pltpu.VMEM((seq_count, drafts, 256), bf16),
            pltpu.VMEM((seq_count, drafts, 256), bf16),
            pltpu.VMEM((seq_count, drafts, 256), bf16),
            pltpu.VMEM((6, drafts, 256), bf16),
            pltpu.SemaphoreType.DMA((4,)),
            pltpu.SemaphoreType.DMA((8, 3)),
            pltpu.SemaphoreType.DMA((8, 3)),
        ],
        compiler_params=pltpu.CompilerParams(
            collective_id=0, has_side_effects=True, vmem_limit_bytes=56 * 1024 * 1024
        ),
        name="tree_attention",
    )(
        tokens, norm_gain.reshape(2, -1), w_query, w_key.T, w_value.T, w_forget.T,
        forget_bias, query_gain.reshape(1, -1), key_gain.reshape(1, -1), w_out,
        key_cache, value_cache, gate_sums, parents.T, lengths, accepted,
    )
    return mixed


def solution(mesh):
    return jax.shard_map(
        body,
        mesh=mesh,
        in_specs=(
            P(None, None, "kv"),
            P("kv"),
            P("kv", "tp"),
            P("kv", "tp"),
            P("kv", "tp"),
            P(),
            P("tp"),
            P(),
            P(),
            P("tp", "kv"),
            P(None, "tp", "kv"),
            P(None, "tp", "kv"),
            P(None, "tp", "kv"),
            P(),
            P(),
            P(),
        ),
        out_specs=P(None, None, "kv"),
        check_vma=False,
    )
```

time: 89.5 us -> 88.7 us (level)
  local copies, waits for them, and re-layouts: 9.8 us -> 1.92 us
  Pallas kernels: 79.3 us -> 86.6 us
    pallas_call x1, Pallas kernels: 79.3 us -> 86.6 us  [body(): pl.pallas_call(kernel, out_shape=jax.ShapeDtypeStruct(tokens.shape, bf16)...]
    unnamed x5 -> x1, local copies, waits for them, and re-layouts: 8.55 us -> 1.92 us
    reshape x1 -> x0, local copies, waits for them, and re-layouts: 1.25 us -> none  [body(): norm_gain.reshape(1, -1)]
where the time goes in v2:
time: 88.7 us; the launch traced here: 88.5 us
  Pallas kernels  86.6 us (98%)
  local copies, waits for them, and re-layouts  1.92 us (2%)
    pallas_call x1, Pallas kernels, body(): pl.pallas_call(kernel, out_shape=jax.ShapeDtypeStruct(tokens.shape, bf16)...  86.6 us
    unnamed x1, local copies, waits for them, and re-layouts  1.92 us

profile of v2, /device:TPU:1, one launch (start us, length us, event | category | flops | bytes accessed | tf_op | source)
XLA Modules:
  0.0 88.5 jit_solution(4530563897722437003)
XLA Ops:
  0.0 86.6 %tree_attention.1 = bf16[48,24,256]{2,1,0:T(8,128)(2,1)} custom-call(bf16[48,24,256]{2,1,0:T(8,128)(2,1)} %tokens.1, bf16[2,128]{1,0:T(2,128)(2,1)} %bitcast.11, bf16[256,256]{1,0:T(8,128)(2,1)} %w_query.1, bf16[64,256]{1,0:T(8,128)(2,1)} %bitcast.8, bf16[64,256]{1,0:T(8,128)(2,1)} %bitcast.9, bf16[32,4096]{1,0:T(8,128)(2,1)} %bitcast.7, f32[4]{0:T(128)} %forget_bias.1, ...), custom_call_target="tpu_custom_call" | custom-call | tf_op jit(solution)/shard_map/tree_attention/pallas_call | solution.py:384
  86.6 1.9 %copy.18 = bf16[48,24,256]{2,1,0:T(8,128)(2,1)} copy(bf16[48,24,256]{2,1,0:T(8,128)(2,1)} %tree_attention.1) | data formatting | bytes 1179648

commit v3 on v2

--- a/solution.py
+++ b/solution.py
@@ -13,6 +13,7 @@
 KV_SIDE = 4
 N_KV = 16
 N_TP = 8
+GROUPS = ((0, 1), (1, 6), (6, 11), (11, 16))
 MESH = pl.DeviceIdType.MESH
 
 PROJ, STAT, QUERY, PART, LSE, ATT, OUT, FINAL = range(8)
@@ -136,7 +137,12 @@
         own_proj[...] = projected[:share]
         return carry
 
-    lax.fori_loop(0, N_KV, lambda i, c: project(N_KV - 1 - i, c), 0)
+    def project_four(i, carry):
+        for k in range(4):
+            project(N_KV - 1 - 4 * i - k, carry)
+        return carry
+
+    lax.fori_loop(0, N_KV // 4, project_four, 0)
 
     pl.semaphore_wait(barrier, N_KV + N_TP - 2)
     for o in range(1, N_KV):
@@ -260,15 +266,19 @@
         o_send[at] = jnp.concatenate(
             [weighted[h * drafts : (h + 1) * drafts] for h in range(heads)], axis=1
         ).astype(bf16)
-        if o > 0:
-            remote(PART, j, o_send.at[at], o_recv.at[at], {"kv": src}).start()
         return jnp.where(wide_lane == o, jnp.concatenate(tops, axis=0) + jnp.log(total), sums)
 
     def attend_all(j, first, last, sums):
-        for o in range(first, last):
-            if o == 1:
+        for start, stop in GROUPS:
+            if start < first or stop > last:
+                continue
+            if start == 1:
                 arrived(QUERY, j, others(q_all, j))
-            sums = attend(j, o, sums)
+            for o in range(start, stop):
+                sums = attend(j, o, sums)
+            for o in range(max(start, 1), stop):
+                at = j * N_KV + o
+                remote(PART, j, o_send.at[at], o_recv.at[at], {"kv": behind(o)}).start()
         if last < N_KV:
             return sums
         table = padded(sums, 128).T
@@ -341,17 +351,17 @@
                 summed = summed + t_recv[j * N_KV + u * 2 + half].astype(f32)
             seq = (tp * 2 + half) * seqs + j
             fin[j * 2 + half] = summed.astype(bf16)
-            out[seq] = summed.astype(bf16)
             for u in range(1, N_TP):
                 remote(FINAL, j, fin.at[j * 2 + half], out.at[seq], {"tp": tp_ahead(u)}).start()
+            pltpu.make_async_copy(fin.at[j * 2 + half], out.at[seq], local_sem.at[4 + j * 2 + half]).start()
 
     none = jnp.zeros((heads * drafts, 128), f32)
     attend_all(0, 0, N_KV, none)
     attend_all(1, 0, N_KV, none)
     merge(0)
-    sums = attend_all(2, 0, 10, none)
+    sums = attend_all(2, 0, 11, none)
     merge(1)
-    attend_all(2, 10, N_KV, sums)
+    attend_all(2, 11, N_KV, sums)
     output(0)
     merge(2)
     output(1)
@@ -361,6 +371,9 @@
     add_up(2)
     for j in range(seqs):
         arrived(FINAL, j, t_recv.at[pl.ds(j * N_KV + 2, N_KV - 2)])
+        for half in range(2):
+            seq = (tp * 2 + half) * seqs + j
+            pltpu.make_async_copy(fin.at[j * 2 + half], out.at[seq], local_sem.at[4 + j * 2 + half]).wait()
     gone(STAT, 0, others(s_send, 0))
     for j in range(seqs):
         gone(PROJ, j, others(p_send, j))
@@ -388,7 +401,7 @@
             vmem, vmem, vmem, vmem, vmem, anywhere, smem, vmem, vmem, vmem,
             anywhere, anywhere, anywhere, smem, smem, smem,
         ],
-        out_specs=vmem,
+        out_specs=anywhere,
         scratch_shapes=[
             pltpu.VMEM((128, local_width), bf16),
             pltpu.VMEM((w_forget.shape[1], local_width), bf16),
@@ -414,7 +427,7 @@
             pltpu.VMEM((seq_count, drafts, 256), bf16),
             pltpu.VMEM((seq_count, drafts, 256), bf16),
             pltpu.VMEM((6, drafts, 256), bf16),
-            pltpu.SemaphoreType.DMA((4,)),
+            pltpu.SemaphoreType.DMA((10,)),
             pltpu.SemaphoreType.DMA((8, 3)),
             pltpu.SemaphoreType.DMA((8, 3)),
         ],

time: 88.7 us -> 66.7 us (0.75)
  Pallas kernels: 86.6 us -> 64.6 us
    pallas_call x1, Pallas kernels: 86.6 us -> 64.6 us  [body(): pl.pallas_call(kernel, out_shape=jax.ShapeDtypeStruct(tokens.shape, bf16)...]
where the time goes in v3:
time: 66.7 us; the launch traced here: 66.6 us
  Pallas kernels  64.6 us (97%)
  local copies, waits for them, and re-layouts  1.92 us (3%)
    pallas_call x1, Pallas kernels, body(): pl.pallas_call(kernel, out_shape=jax.ShapeDtypeStruct(tokens.shape, bf16)...  64.6 us
    unnamed x1, local copies, waits for them, and re-layouts  1.92 us

profile of v3, /device:TPU:1, one launch (start us, length us, event | category | flops | bytes accessed | tf_op | source)
XLA Modules:
  0.0 66.6 jit_solution(9998742032567653346)
XLA Ops:
  0.0 64.6 %tree_attention.1 = bf16[48,24,256]{2,1,0:T(8,128)(2,1)} custom-call(bf16[48,24,256]{2,1,0:T(8,128)(2,1)} %tokens.1, bf16[2,128]{1,0:T(2,128)(2,1)} %bitcast.11, bf16[256,256]{1,0:T(8,128)(2,1)} %w_query.1, bf16[64,256]{1,0:T(8,128)(2,1)} %bitcast.8, bf16[64,256]{1,0:T(8,128)(2,1)} %bitcast.9, bf16[32,4096]{1,0:T(8,128)(2,1)} %bitcast.7, f32[4]{0:T(128)} %forget_bias.1, ...), custom_call_target="tpu_custom_call" | custom-call | tf_op jit(solution)/shard_map/tree_attention/pallas_call | solution.py:397
  64.6 1.9 %copy.18 = bf16[48,24,256]{2,1,0:T(8,128)(2,1)} copy(bf16[48,24,256]{2,1,0:T(8,128)(2,1)} %tree_attention.1) | data formatting | bytes 1179648

commit v4 on v3

--- a/solution.py
+++ b/solution.py
@@ -353,7 +353,7 @@
             fin[j * 2 + half] = summed.astype(bf16)
             for u in range(1, N_TP):
                 remote(FINAL, j, fin.at[j * 2 + half], out.at[seq], {"tp": tp_ahead(u)}).start()
-            pltpu.make_async_copy(fin.at[j * 2 + half], out.at[seq], local_sem.at[4 + j * 2 + half]).start()
+            out[seq] = summed.astype(bf16)
 
     none = jnp.zeros((heads * drafts, 128), f32)
     attend_all(0, 0, N_KV, none)
@@ -366,14 +366,11 @@
     merge(2)
     output(1)
     add_up(0)
+    output(2)
     add_up(1)
-    output(2)
     add_up(2)
     for j in range(seqs):
         arrived(FINAL, j, t_recv.at[pl.ds(j * N_KV + 2, N_KV - 2)])
-        for half in range(2):
-            seq = (tp * 2 + half) * seqs + j
-            pltpu.make_async_copy(fin.at[j * 2 + half], out.at[seq], local_sem.at[4 + j * 2 + half]).wait()
     gone(STAT, 0, others(s_send, 0))
     for j in range(seqs):
         gone(PROJ, j, others(p_send, j))
@@ -396,12 +393,12 @@
     anywhere = pl.BlockSpec(memory_space=pl.ANY)
     mixed = pl.pallas_call(
         kernel,
-        out_shape=jax.ShapeDtypeStruct(tokens.shape, bf16),
+        out_shape=pltpu.VMEM(tokens.shape, bf16),
         in_specs=[
             vmem, vmem, vmem, vmem, vmem, anywhere, smem, vmem, vmem, vmem,
             anywhere, anywhere, anywhere, smem, smem, smem,
         ],
-        out_specs=anywhere,
+        out_specs=vmem,
         scratch_shapes=[
             pltpu.VMEM((128, local_width), bf16),
             pltpu.VMEM((w_forget.shape[1], local_width), bf16),
@@ -432,7 +429,7 @@
             pltpu.SemaphoreType.DMA((8, 3)),
         ],
         compiler_params=pltpu.CompilerParams(
-            collective_id=0, has_side_effects=True, vmem_limit_bytes=56 * 1024 * 1024
+            collective_id=0, has_side_effects=True, vmem_limit_bytes=66350000
         ),
         name="tree_attention",
     )(

time: 66.7 us -> 63.4 us (0.951)
  Pallas kernels: 64.6 us -> 62.4 us
  local copies, waits for them, and re-layouts: 1.92 us -> 0.82 us
    pallas_call x1, Pallas kernels: 64.6 us -> 62.4 us  [body(): pl.pallas_call(kernel, out_shape=pltpu.VMEM(tokens.shape, bf16), in_specs...]
    unnamed x1, local copies, waits for them, and re-layouts: 1.92 us -> 0.82 us
where the time goes in v4:
time: 63.4 us; the launch traced here: 63.2 us
  Pallas kernels  62.4 us (98%)
  local copies, waits for them, and re-layouts  0.82 us (1%)
    pallas_call x1, Pallas kernels, body(): pl.pallas_call(kernel, out_shape=pltpu.VMEM(tokens.shape, bf16), in_specs...  62.4 us

profile of v4, /device:TPU:1, one launch (start us, length us, event | category | flops | bytes accessed | tf_op | source)
XLA Modules:
  0.0 63.2 jit_solution(959820927444539751)
XLA Ops:
  0.0 62.4 %tree_attention.1 = bf16[48,24,256]{2,1,0:T(8,128)(2,1)S(1)} custom-call(bf16[48,24,256]{2,1,0:T(8,128)(2,1)} %tokens.1, bf16[2,128]{1,0:T(2,128)(2,1)} %bitcast.11, bf16[256,256]{1,0:T(8,128)(2,1)} %w_query.1, bf16[64,256]{1,0:T(8,128)(2,1)} %bitcast.8, bf16[64,256]{1,0:T(8,128)(2,1)} %bitcast.9, bf16[32,4096]{1,0:T(8,128)(2,1)} %bitcast.7, f32[4]{0:T(128)} %forget_bias.1, ...), custom_call_target="tpu_custom_call" | custom-call | tf_op jit(solution)/shard_map/tree_attention/pallas_call | solution.py:394
  62.4 0.8 %copy.18 = bf16[48,24,256]{2,1,0:T(8,128)(2,1)} copy(bf16[48,24,256]{2,1,0:T(8,128)(2,1)S(1)} %tree_attention.1) | data formatting | bytes 1179648

commit v5 on v4

--- a/solution.py
+++ b/solution.py
@@ -13,7 +13,7 @@
 KV_SIDE = 4
 N_KV = 16
 N_TP = 8
-GROUPS = ((0, 1), (1, 6), (6, 11), (11, 16))
+GROUPS = ((0, 1), (1, 6), (6, 12), (12, 16))
 MESH = pl.DeviceIdType.MESH
 
 PROJ, STAT, QUERY, PART, LSE, ATT, OUT, FINAL = range(8)
@@ -359,9 +359,8 @@
     attend_all(0, 0, N_KV, none)
     attend_all(1, 0, N_KV, none)
     merge(0)
-    sums = attend_all(2, 0, 11, none)
+    attend_all(2, 0, N_KV, none)
     merge(1)
-    attend_all(2, 11, N_KV, sums)
     output(0)
     merge(2)
     output(1)

time: 63.4 us -> 62.1 us (0.979)
  Pallas kernels: 62.4 us -> 61.1 us
    pallas_call x1, Pallas kernels: 62.4 us -> 61.1 us  [body(): pl.pallas_call(kernel, out_shape=pltpu.VMEM(tokens.shape, bf16), in_specs...]
where the time goes in v5:
time: 62.1 us; the launch traced here: 62 us
  Pallas kernels  61.1 us (98%)
  local copies, waits for them, and re-layouts  0.82 us (1%)
    pallas_call x1, Pallas kernels, body(): pl.pallas_call(kernel, out_shape=pltpu.VMEM(tokens.shape, bf16), in_specs...  61.1 us

profile of v5, /device:TPU:1, one launch (start us, length us, event | category | flops | bytes accessed | tf_op | source)
XLA Modules:
  0.0 62.0 jit_solution(3488234650139212836)
XLA Ops:
  0.0 61.1 %tree_attention.1 = bf16[48,24,256]{2,1,0:T(8,128)(2,1)S(1)} custom-call(bf16[48,24,256]{2,1,0:T(8,128)(2,1)} %tokens.1, bf16[2,128]{1,0:T(2,128)(2,1)} %bitcast.11, bf16[256,256]{1,0:T(8,128)(2,1)} %w_query.1, bf16[64,256]{1,0:T(8,128)(2,1)} %bitcast.8, bf16[64,256]{1,0:T(8,128)(2,1)} %bitcast.9, bf16[32,4096]{1,0:T(8,128)(2,1)} %bitcast.7, f32[4]{0:T(128)} %forget_bias.1, ...), custom_call_target="tpu_custom_call" | custom-call | tf_op jit(solution)/shard_map/tree_attention/pallas_call | solution.py:393
  61.1 0.8 %copy.18 = bf16[48,24,256]{2,1,0:T(8,128)(2,1)} copy(bf16[48,24,256]{2,1,0:T(8,128)(2,1)S(1)} %tree_attention.1) | data formatting | bytes 1179648
